TPU v7x, 32 devices: a whole 2x2x4 slice. The times are simulated.
32 devices in a mesh: ep: 8 (over z, y), tp: 4 (over x, core).
Axes of the slice: x: 2, y: 2, z: 4, core: 2. Of those that a mesh axis runs over, the one named last changes fastest.
Arguments:
- queries: bfloat16 [8192, 1024], P('ep', 'tp'), may hold values from -6 to 6
- keys: bfloat16 [8192, 1024], P('ep', 'tp'), may hold values from -6 to 6
- values: bfloat16 [8192, 2048], P('ep', 'tp'), may hold values from -6 to 6
- log_input_gate: float32 [8192, 8], P('ep', 'tp'), may hold values from -6 to 103
- forget_preactivation: float32 [8192, 8], P('ep', 'tp'), may hold values from 0 to 16
- forget_offset: float32 [8192, 8], P('ep', 'tp'), may hold values from -0.7 to 0
- head_norm_scale: float32 [2048], P('tp'), may hold values from 0.1 to 1.9
- memory_output_weight: bfloat16 [2048, 4096], P('tp'), may hold values from -0.125 to 0.125
- second_micro_tokens: bfloat16 [4096, 4096], P('ep'), may hold values from -6 to 6
- expert_norm_scale: float32 [4096], replicated, may hold values from 0.1 to 1.9
- expert_choice_index: int32 [4096, 2], P('ep'), may hold values from 0 to 15, all different within a row; in each aligned block of 512 rows (0 to 511, 512 to 1023, ...) at most 96 rows name the same one
- group_likelihood: float32 [4096], P('ep'), may hold values from 0.2 to 1
- expert_raw_weight: float32 [4096, 2], P('ep'), may hold values from 0.1 to 1
- gate_weight: bfloat16 [16, 4096, 1024], P('ep', None, 'tp'), may hold values from -0.09375 to 0.09375
- up_weight: bfloat16 [16, 4096, 1024], P('ep', None, 'tp'), may hold values from -0.09375 to 0.09375
- down_weight: bfloat16 [16, 1024, 4096], P('ep', 'tp'), may hold values from -0.1875 to 0.1875
Outputs:
- mixed: bfloat16 [8192, 4096], P(('ep', 'tp'))
- routed: bfloat16 [4096, 4096], P('ep', 'tp')
Inputs may be any that keep to these rules, and one draw needn't show every extreme that they name: `expert_choice_index`: each row names 2 different experts. Within the 512 rows of one index of ep (aligned blocks) no expert is named more than 96 times, and in some blocks one expert is named exactly 96 times.
All inputs are finite; a program needn't handle non-finite values.
Results may differ from a plain program's by a relative error of at most 0.012.
Values may be sent and summed in bfloat16 or wider, within the bound.
A program may use at most 192 MiB of HBM per device.

v0:
```python
import math
import jax
import jax.numpy as jnp
from jax import lax
from jax.sharding import PartitionSpec as P

BLOCK = 128
EPSILON = 1e-06
FLOOR_LOG = -1e30


def carried_in(value, axis, join, neutral):
    count, mine = (lax.axis_size(axis), lax.axis_index(axis))
    pieces = jax.tree.map(lambda part: lax.all_gather(part, axis), value)
    subtotal = jax.tree.map(
        lambda part, zero: jnp.full_like(part, 0) + jnp.asarray(zero, part.dtype), value, neutral
    )

    def turn(position, subtotal):
        longer = join(subtotal, jax.tree.map(lambda part: part[position], pieces))
        return jax.tree.map(lambda new, old: jnp.where(position < mine, new, old), longer, subtotal)

    return lax.fori_loop(0, count - 1, turn, subtotal)


def merge_states(earlier, later):
    memory_one, stable_one, total_one = earlier
    memory_two, stable_two, total_two = later
    highest = jnp.maximum(total_two + stable_one, stable_two)
    weight_one = jnp.exp(total_two + stable_one - highest)
    weight_two = jnp.exp(stable_two - highest)
    memory = weight_one[..., None, None] * memory_one + weight_two[..., None, None] * memory_two
    return (memory, highest, total_one + total_two)


def advance(carry, piece):
    return (merge_states(carry, piece), carry)


def recurrence_portion(
    queries,
    keys,
    values,
    log_input_gate,
    forget_preactivation,
    forget_offset,
    head_norm_scale,
    memory_output_weight,
):
    row_count, head_count = log_input_gate.shape
    key_width = queries.shape[1] // head_count
    value_width = values.shape[1] // head_count
    block_count = row_count // BLOCK
    qk_scale = 1.0 / math.sqrt(key_width)
    query_blocks = queries.reshape(block_count, BLOCK, head_count, key_width)
    key_blocks = keys.reshape(block_count, BLOCK, head_count, key_width)
    value_blocks = values.reshape(block_count, BLOCK, head_count, value_width)
    key_float = key_blocks.astype(jnp.float32) * qk_scale
    forget_log_factor = jax.nn.log_sigmoid(forget_preactivation) + forget_offset
    forget_log_factor = forget_log_factor.reshape(block_count, BLOCK, head_count).transpose(0, 2, 1)
    in_gate = log_input_gate.reshape(block_count, BLOCK, head_count).transpose(0, 2, 1)
    running = jnp.cumsum(forget_log_factor, axis=-1)
    totals = running[..., -1]
    to_end = totals[..., None] - running + in_gate
    block_peak = jnp.max(to_end, axis=-1)
    key_weight = jnp.exp(to_end - block_peak[..., None])
    weighted_keys = (key_float * key_weight.transpose(0, 2, 1)[..., None]).astype(jnp.bfloat16)
    block_memory = jnp.einsum(
        "bshd,bshe->bhde", weighted_keys, value_blocks, preferred_element_type=jnp.float32
    )
    empty = (
        jnp.zeros((head_count, key_width, value_width), jnp.float32),
        jnp.full((head_count,), FLOOR_LOG, jnp.float32),
        jnp.zeros((head_count,), jnp.float32),
    )
    device_state, starts = lax.scan(advance, empty, (block_memory, block_peak, totals))
    incoming = carried_in(device_state, "ep", merge_states, empty)
    memory, peak, unused = merge_states(incoming, starts)
    scores = (
        jnp.einsum("bthd,bshd->bhts", query_blocks, key_blocks, preferred_element_type=jnp.float32)
        * qk_scale
    )
    causal = jnp.tril(jnp.ones((BLOCK, BLOCK), dtype=bool))
    log_weight = running[..., :, None] - running[..., None, :] + in_gate[..., None, :]
    log_weight = jnp.where(causal, log_weight, -jnp.inf)
    carried = running + peak[..., None]
    stable = jnp.maximum(carried, jnp.max(log_weight, axis=-1))
    inner = (scores * jnp.exp(log_weight - stable[..., None])).astype(jnp.bfloat16)
    outer = jnp.exp(carried - stable)
    memory_half = memory.astype(jnp.bfloat16)
    state = outer[..., None] * jnp.einsum(
        "bthd,bhde->bhte", query_blocks, memory_half, preferred_element_type=jnp.float32
    )
    state = state + jnp.einsum(
        "bhts,bshe->bhte", inner, value_blocks, preferred_element_type=jnp.float32
    )
    state = state * lax.rsqrt(jnp.mean(state * state, axis=-1, keepdims=True) + EPSILON)
    hidden = state.transpose(0, 2, 1, 3).reshape(row_count, head_count * value_width)
    hidden = (hidden * head_norm_scale).astype(jnp.bfloat16)
    return lax.psum_scatter(
        jnp.dot(hidden, memory_output_weight, preferred_element_type=jnp.float32).astype(
            jnp.bfloat16
        ),
        "tp",
        scatter_dimension=0,
        tiled=True,
    )


def expert_half(
    second_micro_tokens,
    expert_norm_scale,
    expert_choice_index,
    group_likelihood,
    expert_raw_weight,
    gate_weight,
    up_weight,
    down_weight,
):
    token_count, model_width = second_micro_tokens.shape
    pick_count = expert_choice_index.shape[1]
    local_experts = gate_weight.shape[0]
    ep_size = lax.axis_size("ep")
    tp_size = lax.axis_size("tp")
    expert_count = local_experts * ep_size
    capacity = tp_size * max(1, 3 * pick_count * token_count // (2 * expert_count * tp_size))
    token_float = second_micro_tokens.astype(jnp.float32)
    normed = token_float * lax.rsqrt(
        jnp.mean(token_float * token_float, axis=-1, keepdims=True) + EPSILON
    )
    normed = (normed * expert_norm_scale).astype(jnp.bfloat16)
    share = expert_raw_weight / jnp.sum(expert_raw_weight, axis=1, keepdims=True)
    route_weight = group_likelihood[:, None] * share
    flat_expert = expert_choice_index.reshape(-1)
    one_hot = (flat_expert[:, None] == jnp.arange(expert_count, dtype=jnp.int32)[None, :]).astype(
        jnp.int32
    )
    slot_rank = jnp.sum(jnp.cumsum(one_hot, axis=0) * one_hot, axis=1) - 1
    owner = flat_expert // local_experts
    local_index = flat_expert % local_experts
    slot_index = owner * (local_experts * capacity) + local_index * capacity + slot_rank
    slot_total = local_experts * ep_size * capacity
    token_index = jnp.arange(token_count * pick_count, dtype=jnp.int32) // pick_count
    slot_token = jnp.zeros((slot_total,), jnp.int32).at[slot_index].set(token_index)
    slot_used = jnp.zeros((slot_total,), bool).at[slot_index].set(True)
    outgoing = jnp.where(slot_used[:, None], normed[slot_token], jnp.zeros((), jnp.bfloat16))
    outgoing = outgoing.reshape(ep_size, local_experts, capacity, model_width)
    quarter = capacity // tp_size
    own_share = lax.dynamic_slice_in_dim(outgoing, lax.axis_index("tp") * quarter, quarter, 2)
    arrived = lax.all_to_all(own_share, "ep", split_axis=0, concat_axis=0, tiled=True)
    expert_arrived = lax.all_gather(arrived, "tp", axis=2, tiled=True)
    gate = jnp.einsum(
        "serd,edf->serf", expert_arrived, gate_weight, preferred_element_type=jnp.float32
    )
    upward = jnp.einsum(
        "serd,edf->serf", expert_arrived, up_weight, preferred_element_type=jnp.float32
    )
    hidden = (jax.nn.silu(gate) * upward).astype(jnp.bfloat16)
    summed = lax.psum_scatter(
        jnp.einsum(
            "serf,efc->cser", hidden, down_weight, preferred_element_type=jnp.float32
        ).astype(jnp.bfloat16),
        "tp",
        scatter_dimension=0,
        tiled=True,
    )
    returned = lax.all_to_all(summed, "ep", split_axis=1, concat_axis=1, tiled=True)
    flat_result = returned.reshape(returned.shape[0], slot_total)
    picked = jnp.take(flat_result, slot_index, axis=1).astype(jnp.float32)
    picked = picked.reshape(flat_result.shape[0], token_count, pick_count)
    combined = jnp.sum(picked * route_weight[None], axis=2)
    return combined.T.astype(jnp.bfloat16)


def per_device(
    queries,
    keys,
    values,
    log_input_gate,
    forget_preactivation,
    forget_offset,
    head_norm_scale,
    memory_output_weight,
    second_micro_tokens,
    expert_norm_scale,
    expert_choice_index,
    group_likelihood,
    expert_raw_weight,
    gate_weight,
    up_weight,
    down_weight,
):
    mixed = recurrence_portion(
        queries,
        keys,
        values,
        log_input_gate,
        forget_preactivation,
        forget_offset,
        head_norm_scale,
        memory_output_weight,
    )
    routed = expert_half(
        second_micro_tokens,
        expert_norm_scale,
        expert_choice_index,
        group_likelihood,
        expert_raw_weight,
        gate_weight,
        up_weight,
        down_weight,
    )
    return (mixed, routed)


def solution(mesh):
    in_specs = (
        P("ep", "tp"),
        P("ep", "tp"),
        P("ep", "tp"),
        P("ep", "tp"),
        P("ep", "tp"),
        P("ep", "tp"),
        P("tp"),
        P("tp", None),
        P("ep", None),
        P(),
        P("ep", None),
        P("ep"),
        P("ep", None),
        P("ep", None, "tp"),
        P("ep", None, "tp"),
        P("ep", "tp", None),
    )
    out_specs = (P(("ep", "tp"), None), P("ep", "tp"))
    return jax.shard_map(
        per_device, mesh=mesh, in_specs=in_specs, out_specs=out_specs, check_vma=False
    )
```

profile of v0, /device:TPU:0, one launch (start us, length us, event | category | flops | bytes accessed | tf_op | source)
XLA Modules:
  0.0 474.5 jit_solution(9666437804469296286)
XLA Ops:
  7.2 0.8 copy.132
  8.6 3.1 fusion.13
  11.7 4.5 reduce-window.6
  16.7 4.3 scatter_custom_fusion.1
  21.1 4.5 scatter_custom_fusion
  25.7 5.8 %fusion.15 = bf16[512,4096]{1,0:T(8,128)(2,1)} fusion(bf16[512,4096]{1,0:T(8,128)(2,1)} %param.28, f32[4096]{0:T(1024)S(1)} %copy-done.6, f32[512]{0:T(512)S(1)} %add_rsqrt_fusion), kind=kLoop, calls=%fused_computation.37 | loop fusion | flops 8388608 | bytes 8407040 | tf_op jit(solution)/shard_map/convert_element_type | solution.py:131
  31.5 24.8 %gather_fusion = bf16[1536,4096]{1,0:T(8,128)(2,1)} fusion(bf16[512,4096]{1,0:T(8,128)(2,1)} %fusion.15, s32[2048]{0:T(1024)S(1)} %pad_clamp_fusion), kind=kCustom, calls=%fused_computation | custom fusion | bytes 25171968 | tf_op jit(solution)/shard_map/gather | solution.py:146
  56.3 2.8 dynamic-slice_select_fusion
  59.2 77.8 %all_to_all.10 = bf16[8,2,24,4096]{3,2,1,0:T(8,128)(2,1)S(1)} all-to-all(bf16[8,2,24,4096]{3,2,1,0:T(8,128)(2,1)S(1)} %dynamic-slice_select_fusion), channel_id=1, replica_groups=mesh['ep'=8,'tp'=4] {'ep'}, dimensions={0} | all-to-all | bytes 6291456 | tf_op jit(solution)/shard_map/all_to_all | solution.py:150
  137.0 1.9 copy.139
  141.1 1.1 copy.110
  142.3 1.5 fusion.44
  143.8 7.7 %while.37 = (s32[]{:T(128)}, f32[2,128,256]{2,1,0:T(8,128)S(1)}, f32[2]{0:T(128)S(1)}, f32[2]{0:T(128)S(1)}, f32[8,2,128,256]{3,2,1,0:T(8,128)}, /*index=5*/f32[...) while((s32[]{:T(128)}, f32[2,128,256]{2,1,0:T(8,128)S(1)}, ...), condition=%wide.region_3.4_spmd.clone, body=%wide.region_2.3_spmd.clone.sunk | while | flops 327699 | bytes 1311034 | solution.py:76
  143.8 0.7 bitcast_dynamic-update-slice_fusion.2
  144.7 0.7 bitcast_dynamic-update-slice_fusion.2
  145.7 0.7 bitcast_dynamic-update-slice_fusion.2
  146.7 0.7 bitcast_dynamic-update-slice_fusion.2
  147.6 0.7 bitcast_dynamic-update-slice_fusion.2
  148.6 0.7 bitcast_dynamic-update-slice_fusion.2
  149.5 0.7 bitcast_dynamic-update-slice_fusion.2
  152.5 67.7 %all-gather.6.cloned.1.call-done = bf16[8,2,96,4096]{3,2,0,1:T(8,128)(2,1)} async-done(((bf16[8,2,24,4096]{3,2,0,1:T(8,128)(2,1)}), bf16[8,2,96,4096]{3,2,0,1:T(8,128)(2,1)}) %all-gather.6.cloned.1.call-update) | async-done | bytes 12582928 | tf_op jit(solution)/shard_map/all_gather | solution.py:151
  220.2 7.8 %fusion.19 = f32[2,8,96,256]{3,2,1,0:T(8,128)S(1)} fusion(bf16[8,2,96,4096]{3,2,0,1:T(8,128)(2,1)} %all-gather.6.cloned.1.call-done, bf16[2,4096,256]{2,1,0:T(8,128)(2,1)} %param.33), kind=kOutput, calls=%fused_computation.42 | convolution fusion | flops 3221225472 | bytes 18350080 | tf_op jit(solution)/shard_map/serd,edf->serf/dot_general | solution.py:152
  228.0 8.7 %fusion.25 = bf16[8,2,96,256]{3,2,0,1:T(8,128)(2,1)S(1)} fusion(f32[2,8,96,256]{3,2,1,0:T(8,128)S(1)} %fusion.19, bf16[8,2,96,4096]{3,2,0,1:T(8,128)(2,1)} %all-gather.6.cloned.1.call-done, bf16[2,4096,256]{2,1,0:T(8,128)(2,1)S(1)} %copy-done.12), kind=kOutput, calls=%fused_computation.57 | convolution fusion | flops 3223584768 | bytes 19136512 | tf_op jit(solution)/shard_map/serd,edf->serf/dot_general | solution.py:155
  236.7 6.4 %convert_bitcast_fusion = bf16[4096,8,2,96]{0,3,1,2:T(8,128)(2,1)} fusion(bf16[8,2,96,256]{3,2,0,1:T(8,128)(2,1)S(1)} %fusion.25, bf16[2,256,4096]{2,1,0:T(8,128)(2,1)S(1)} %copy-done.1), kind=kOutput, calls=%fused_computation.32 | convolution fusion | flops 3227516928 | bytes 17563648 | tf_op jit(solution)/shard_map/serf,efc->cser/dot_general | solution.py:160
  245.4 22.1 %all-reduce.2 = (f32[16]{0:T(128)S(1)}, f32[16]{0:T(128)S(1)}) all-reduce(f32[16]{0:T(128)S(1)} %dynamic-update-slice, f32[16]{0:T(128)S(1)} %dynamic-update-slice.1), channel_id=2, replica_groups=mesh['ep'=8,'tp'=4] {'ep'}, use_global_device_ids=true, to_apply=%add | all-reduce | flops 32 | bytes 256
  267.7 1.0 reshape.247
  269.4 2.7 all-gather.8.cloned.1.call-done
  272.1 8.0 %while.38 = (s32[]{:T(128)}, f32[2,128,256]{2,1,0:T(8,128)S(1)}, f32[2]{0:T(128)S(1)}, s32[]{:T(128)}, f32[8,2]{1,0:T(8,128)S(1)}, /*index=5*/f32[8,2]{1,0:T(8,1...) while((s32[]{:T(128)}, f32[2,128,256]{2,1,0:T(8,128)S(1)}, f32[2]{0:T(128)S(1)}, s32[]{:T(128)}, ...), condition=%wide.region_5.6_spmd.clone, body=%wide.region_4.5_spmd.clone.sunk | while | flops 327698 | bytes 786655 | solution.py:23
  272.1 1.1 fusion.96
  273.2 1.1 fusion.96
  274.4 1.1 fusion.96
  275.5 1.1 fusion.96
  276.6 1.1 fusion.96
  277.8 1.1 fusion.96
  279.0 1.1 fusion.96
  280.4 3.0 fusion.34
  283.3 4.3 fusion.23
  287.7 2.7 fusion.24
  290.4 1.2 copy.131
  291.6 1.2 copy-done.13
  292.8 7.8 %convolution_convert_fusion = bf16[1024,4096]{1,0:T(8,128)(2,1)} fusion(bf16[512,4096]{1,0:T(8,128)(2,1)S(1)} %copy-done.13, f32[64,8,8,128]{3,2,1,0:T(8,128)S(1)} %bitcast.194, f32[512]{0:T(512)S(1)} %copy-done.14), kind=kOutput, calls=%fused_computation.38 | convolution fusion | flops 4300210176 | bytes 14682112 | tf_op jit(solution)/shard_map/dot_general | solution.py:101
  300.6 69.7 %reduce-scatter.5.cloned.1.call-done = bf16[1024,8,2,96]{0,3,1,2:T(8,128)(2,1)} async-done(((bf16[4096,8,2,96]{0,3,1,2:T(8,128)(2,1)}), bf16[1024,8,2,96]{0,3,1,2:T(8,128)(2,1)}) %reduce-scatter.5.cloned.1.call-update) | async-done | bytes 3145744 | tf_op jit(solution)/shard_map/reduce_scatter | solution.py:159
  370.3 4.0 copy.140
  374.3 5.6 %all-to-all-start.1 = ((bf16[1024,8,2,96]{0,3,2,1:T(8,128)(2,1)}), bf16[1024,8,2,96]{0,3,2,1:T(8,128)(2,1)S(1)}, u32[]{:S(2)}, u32[]{:S(2)}) async-start(bf16[1024,8,2,96]{0,3,2,1:T(8,128)(2,1)} %copy.140), calls=%async_computation.3 | async-start | bytes 6291456 | tf_op jit(solution)/shard_map/all_to_all | solution.py:167
  380.7 69.8 %all-to-all-done.1 = bf16[1024,8,2,96]{0,3,2,1:T(8,128)(2,1)S(1)} async-done(((bf16[1024,8,2,96]{0,3,2,1:T(8,128)(2,1)}), bf16[1024,8,2,96]{0,3,2,1:T(8,128)(2,1)S(1)}, u32[]{:S(2)}, u32[]{:S(2)}) %all-to-all-start.1) | async-done | bytes 3145760 | tf_op jit(solution)/shard_map/all_to_all | solution.py:167
  450.4 5.4 %gather_fusion.1 = bf16[1024,1024]{1,0:T(8,128)(2,1)} fusion(bf16[1024,1536]{0,1:T(8,128)(2,1)S(1)} %bitcast.191, s32[1024]{0:T(1024)S(1)} %broadcast_clamp_fusion), kind=kCustom, calls=%fused_computation.1 | custom fusion | bytes 4198400 | tf_op jit(solution)/shard_map/jit(_take)/gather | solution.py:169
  455.8 2.7 gather.14
  458.6 9.4 %multiply_reduce_fusion = bf16[1024,512]{0,1:T(8,128)(2,1)} fusion(bf16[1024,512,2]{0,2,1:T(2,128)(2,1)S(1)} %gather.14, pred[512,2]{1,0:T(8,128)(4,1)S(1)} %copy.137, f32[512,2]{1,0:T(8,128)S(1)} %copy.141), kind=kLoop, calls=%fused_computation.44 | loop fusion | flops 3670016 | bytes 3150848 | tf_op jit(solution)/shard_map/reduce_sum | solution.py:171
  (171 shorter events, 10.7 us)
Async XLA Ops:
  7.2 213.0 %all-gather.6.cloned.1.call-start = ((), (), s32[]{:S(2)}) async-start(), calls=%async_computation.5 | async-start | bytes 15728640 | tf_op jit(solution)/shard_map/all_gather | solution.py:151
  8.6 17.1 %copy-start.6 = (f32[4096]{0:T(1024)S(1)}, f32[4096]{0:T(1024)}, u32[]{:S(2)}) copy-start(f32[4096]{0:T(1024)} %param.29) | copy-start | bytes 49156
  138.9 0.7 copy-start.9
  138.9 0.7 copy-start.10
  138.9 1.6 copy-start.5
  138.9 1.8 copy-start.2
  138.9 2.1 copy-start.3
  138.9 133.2 %all-gather.8.cloned.1.call-start = ((), (), s32[]{:S(2)}) async-start(), calls=%async_computation.7 | async-start | bytes 2359296 | tf_op jit(solution)/shard_map/all_gather | solution.py:14
  151.5 0.7 copy-start
  152.2 218.1 %reduce-scatter.5.cloned.1.call-start = ((), (), s32[]{:S(2)}) async-start(), calls=%async_computation.6 | async-start | bytes 15728640 | tf_op jit(solution)/shard_map/reduce_scatter | solution.py:159
  220.2 7.8 %copy-start.12 = (bf16[2,4096,256]{2,1,0:T(8,128)(2,1)S(1)}, bf16[2,4096,256]{2,1,0:T(8,128)(2,1)}, u32[]{:S(2)}) copy-start(bf16[2,4096,256]{2,1,0:T(8,128)(2,1)} %param.34) | copy-start | bytes 12582916
  228.0 8.7 %copy-start.1 = (bf16[2,256,4096]{2,1,0:T(8,128)(2,1)S(1)}, bf16[2,256,4096]{2,1,0:T(8,128)(2,1)}, u32[]{:S(2)}) copy-start(bf16[2,256,4096]{2,1,0:T(8,128)(2,1)} %param.35) | copy-start | bytes 12582916
  243.1 0.7 copy-start.15
  243.1 24.7 %copy-start.4 = (bf16[1024,256]{1,0:T(8,128)(2,1)S(1)}, bf16[1024,256]{1,0:T(8,128)(2,1)}, u32[]{:S(2)}) copy-start(bf16[1024,256]{1,0:T(8,128)(2,1)} %param.20) | copy-start | bytes 1572868
  243.1 224.9 %reduce-scatter.3.cloned.1.call-start = ((), (), s32[]{:S(2)}) async-start(), calls=%async_computation.4 | async-start | bytes 10485760 | tf_op jit(solution)/shard_map/reduce_scatter | solution.py:100
  287.6 4.0 copy-start.14
  290.4 2.4 copy-start.13
  374.2 6.0 %copy-start.7 = (s32[512,2]{0,1:T(2,128)S(1)}, s32[512,2]{0,1:T(2,128)}, u32[]{:S(2)}) copy-start(s32[512,2]{0,1:T(2,128)} %param.30) | copy-start | bytes 12292
  374.2 6.2 %copy-start.8 = (f32[512,2]{0,1:T(2,128)S(1)}, f32[512,2]{0,1:T(2,128)}, u32[]{:S(2)}) copy-start(f32[512,2]{0,1:T(2,128)} %param.32) | copy-start | bytes 12292
  374.3 6.2 %copy-start.11 = (f32[512]{0:T(512)S(1)}, f32[512]{0:T(512)}, u32[]{:S(2)}) copy-start(f32[512]{0:T(512)} %param.31) | copy-start | bytes 6148
  374.3 76.2 %all-to-all-start.1 = ((bf16[1024,8,2,96]{0,3,2,1:T(8,128)(2,1)}), bf16[1024,8,2,96]{0,3,2,1:T(8,128)(2,1)S(1)}, u32[]{:S(2)}, u32[]{:S(2)}) async-start(bf16[1024,8,2,96]{0,3,2,1:T(8,128)(2,1)} %copy.140), calls=%async_computation.3 | async-start | bytes 6291456 | tf_op jit(solution)/shard_map/all_to_all | solution.py:167
Sparse Core Ops, SparseCore 0:
  139.1 81.0 all-gather.5
  222.3 49.7 all-gather.7
  274.7 95.5 reduce-scatter.4
  373.3 71.3 reduce-scatter.2
where the time goes:
time: 475 us
  waiting for transfers between devices  210 us (44%)
  blocking collectives  99.9 us (21%)
  local copies, waits for them, and re-layouts  58.9 us (12%)
  other arithmetic  45.1 us (9%)
  matrix products  39.4 us (8%)
  between operations  14.9 us (3%)
  starting transfers between devices  6.03 us (1%)
    all_to_all x1, blocking collectives, expert_half(): lax.all_to_all(own_share, 'ep', split_axis=0, concat_axis=0, tiled=True)  77.8 us
    all_to_all x1, waiting for transfers between devices, expert_half(): lax.all_to_all(summed, 'ep', split_axis=1, concat_axis=1, tiled=True)  69.8 us
    reduce_scatter x1, waiting for transfers between devices, expert_half(): lax.psum_scatter(jnp.einsum('serf,efc->cser', hidden, down_weight, prefer...  69.7 us
    all_gather x1, waiting for transfers between devices, expert_half(): expert_arrived = lax.all_gather(arrived, 'tp', axis=2, tiled=True)  67.7 us
    gather x1, local copies, waits for them, and re-layouts, expert_half(): normed[slot_token]  24.8 us
    unnamed x1, blocking collectives  22.1 us
  transfers between devices with their start and end apart: 5, of which 4 were waited for; matrix products, arithmetic and copies ran while one was open for 18% of the time, Pallas kernels for 0%

commit v1 on v0

--- a/solution.py
+++ b/solution.py
@@ -164,7 +164,9 @@
         scatter_dimension=0,
         tiled=True,
     )
-    returned = lax.all_to_all(summed, "ep", split_axis=1, concat_axis=1, tiled=True)
+    parts = jnp.split(summed, lax.axis_size("ep"), axis=1)
+    received = lax.all_to_all(jnp.stack(parts), "ep", 0, 0)
+    returned = jnp.concatenate(received, axis=1)
     flat_result = returned.reshape(returned.shape[0], slot_total)
     picked = jnp.take(flat_result, slot_index, axis=1).astype(jnp.float32)
     picked = picked.reshape(flat_result.shape[0], token_count, pick_count)

time: 475 us -> 486 us (1.023)
  local copies, waits for them, and re-layouts: 58.9 us -> 69.4 us
    unnamed x42 -> x49, local copies, waits for them, and re-layouts: 5.13 us -> 17.7 us
  transfers between devices with their start and end apart: 5 -> 5, of which waited for: 4 -> 4; matrix products, arithmetic and copies ran while one was open for 18% -> 20% of each run, Pallas kernels for 0% -> 0%
where the time goes in v1:
time: 486 us; the launch traced here: 485 us
  waiting for transfers between devices  210 us (43%)
  blocking collectives  99.9 us (21%)
  local copies, waits for them, and re-layouts  69.4 us (14%)
  other arithmetic  45.1 us (9%)
  matrix products  39.3 us (8%)
  between operations  14.9 us (3%)
  starting transfers between devices  5.96 us (1%)
    all_to_all x1, blocking collectives, expert_half(): lax.all_to_all(own_share, 'ep', split_axis=0, concat_axis=0, tiled=True)  77.8 us
    all_to_all x1, waiting for transfers between devices, expert_half(): received = lax.all_to_all(jnp.stack(parts), 'ep', 0, 0)  69.9 us
    reduce_scatter x1, waiting for transfers between devices, expert_half(): lax.psum_scatter(jnp.einsum('serf,efc->cser', hidden, down_weight, prefer...  69.7 us
    all_gather x1, waiting for transfers between devices, expert_half(): expert_arrived = lax.all_gather(arrived, 'tp', axis=2, tiled=True)  67.6 us
    gather x1, local copies, waits for them, and re-layouts, expert_half(): normed[slot_token]  24.8 us
    unnamed x1, blocking collectives  22.1 us
    unnamed x49, local copies, waits for them, and re-layouts  17.7 us
  transfers between devices with their start and end apart: 5, of which 4 were waited for; matrix products, arithmetic and copies ran while one was open for 20% of the time, Pallas kernels for 0%

profile of v1, /device:TPU:0, one launch (start us, length us, event | category | flops | bytes accessed | tf_op | source)
XLA Modules:
  0.0 485.0 jit_solution(6895762600064794574)
XLA Ops:
  7.2 0.8 copy.151
  8.6 4.5 reduce-window.6
  13.6 4.3 scatter_custom_fusion
  18.1 4.5 scatter_custom_fusion.1
  22.6 3.1 fusion.13
  25.8 5.8 %fusion.15 = bf16[512,4096]{1,0:T(8,128)(2,1)} fusion(bf16[512,4096]{1,0:T(8,128)(2,1)} %param.28, f32[4096]{0:T(1024)S(1)} %copy-done.6, f32[512]{0:T(512)S(1)} %add_rsqrt_fusion), kind=kLoop, calls=%fused_computation.37 | loop fusion | flops 8388608 | bytes 8407040 | tf_op jit(solution)/shard_map/convert_element_type | solution.py:131
  31.6 24.8 %gather_fusion = bf16[1536,4096]{1,0:T(8,128)(2,1)} fusion(bf16[512,4096]{1,0:T(8,128)(2,1)} %fusion.15, s32[2048]{0:T(1024)S(1)} %pad_clamp_fusion), kind=kCustom, calls=%fused_computation | custom fusion | bytes 25171968 | tf_op jit(solution)/shard_map/gather | solution.py:146
  56.3 2.8 dynamic-slice_select_fusion
  59.2 77.8 %all_to_all.10 = bf16[8,2,24,4096]{3,2,1,0:T(8,128)(2,1)S(1)} all-to-all(bf16[8,2,24,4096]{3,2,1,0:T(8,128)(2,1)S(1)} %dynamic-slice_select_fusion), channel_id=1, replica_groups=mesh['ep'=8,'tp'=4] {'ep'}, dimensions={0} | all-to-all | bytes 6291456 | tf_op jit(solution)/shard_map/all_to_all | solution.py:150
  137.0 1.9 copy.158
  140.9 1.1 copy.129
  142.3 1.5 fusion.44
  143.8 7.8 %while.37 = (s32[]{:T(128)}, f32[2,128,256]{2,1,0:T(8,128)S(1)}, f32[2]{0:T(128)S(1)}, f32[2]{0:T(128)S(1)}, f32[8,2,128,256]{3,2,1,0:T(8,128)}, /*index=5*/f32[...) while((s32[]{:T(128)}, f32[2,128,256]{2,1,0:T(8,128)S(1)}, ...), condition=%wide.region_3.4_spmd.clone, body=%wide.region_2.3_spmd.clone.sunk | while | flops 327699 | bytes 1311534 | solution.py:76
  152.6 67.6 %all-gather.6.cloned.1.call-done = bf16[8,2,96,4096]{3,2,0,1:T(8,128)(2,1)} async-done(((bf16[8,2,24,4096]{3,2,0,1:T(8,128)(2,1)}), bf16[8,2,96,4096]{3,2,0,1:T(8,128)(2,1)}) %all-gather.6.cloned.1.call-update) | async-done | bytes 12582928 | tf_op jit(solution)/shard_map/all_gather | solution.py:151
  220.2 7.8 %fusion.19 = f32[2,8,96,256]{3,2,1,0:T(8,128)S(1)} fusion(bf16[8,2,96,4096]{3,2,0,1:T(8,128)(2,1)} %all-gather.6.cloned.1.call-done, bf16[2,4096,256]{2,1,0:T(8,128)(2,1)} %param.33), kind=kOutput, calls=%fused_computation.42 | convolution fusion | flops 3221225472 | bytes 18350080 | tf_op jit(solution)/shard_map/serd,edf->serf/dot_general | solution.py:152
  228.0 8.7 %fusion.25 = bf16[8,2,96,256]{3,2,0,1:T(8,128)(2,1)S(1)} fusion(f32[2,8,96,256]{3,2,1,0:T(8,128)S(1)} %fusion.19, bf16[8,2,96,4096]{3,2,0,1:T(8,128)(2,1)} %all-gather.6.cloned.1.call-done, bf16[2,4096,256]{2,1,0:T(8,128)(2,1)S(1)} %copy-done.12), kind=kOutput, calls=%fused_computation.57 | convolution fusion | flops 3223584768 | bytes 19136512 | tf_op jit(solution)/shard_map/serd,edf->serf/dot_general | solution.py:155
  236.7 6.4 %convert_bitcast_fusion = bf16[4096,8,2,96]{0,3,1,2:T(8,128)(2,1)} fusion(bf16[8,2,96,256]{3,2,0,1:T(8,128)(2,1)S(1)} %fusion.25, bf16[2,256,4096]{2,1,0:T(8,128)(2,1)S(1)} %copy-done.1), kind=kOutput, calls=%fused_computation.32 | convolution fusion | flops 3227516928 | bytes 17563648 | tf_op jit(solution)/shard_map/serf,efc->cser/dot_general | solution.py:160
  245.4 22.1 %all-reduce.2 = (f32[16]{0:T(128)S(1)}, f32[16]{0:T(128)S(1)}) all-reduce(f32[16]{0:T(128)S(1)} %dynamic-update-slice, f32[16]{0:T(128)S(1)} %dynamic-update-slice.1), channel_id=2, replica_groups=mesh['ep'=8,'tp'=4] {'ep'}, use_global_device_ids=true, to_apply=%add | all-reduce | flops 32 | bytes 256
  267.7 1.0 reshape.247
  269.4 2.7 all-gather.8.cloned.1.call-done
  272.1 8.0 %while.38 = (s32[]{:T(128)}, f32[2,128,256]{2,1,0:T(8,128)S(1)}, f32[2]{0:T(128)S(1)}, s32[]{:T(128)}, f32[8,2]{1,0:T(8,128)S(1)}, /*index=5*/f32[8,2]{1,0:T(8,1...) while((s32[]{:T(128)}, f32[2,128,256]{2,1,0:T(8,128)S(1)}, f32[2]{0:T(128)S(1)}, s32[]{:T(128)}, ...), condition=%wide.region_5.6_spmd.clone, body=%wide.region_4.5_spmd.clone.sunk | while | flops 327698 | bytes 786647 | solution.py:23
  272.1 1.1 fusion.104
  273.2 1.1 fusion.104
  274.3 1.1 fusion.104
  275.5 1.1 fusion.104
  276.6 1.1 fusion.104
  277.7 1.1 fusion.104
  278.9 1.1 fusion.104
  280.3 2.9 fusion.34
  283.2 4.2 fusion.23
  287.5 2.7 fusion.24
  290.2 1.2 copy.150
  291.5 1.2 copy-done.13
  292.7 7.8 %convolution_convert_fusion = bf16[1024,4096]{1,0:T(8,128)(2,1)} fusion(bf16[512,4096]{1,0:T(8,128)(2,1)S(1)} %copy-done.13, f32[64,8,8,128]{3,2,1,0:T(8,128)S(1)} %bitcast.242, f32[512]{0:T(512)S(1)} %copy-done.14), kind=kOutput, calls=%fused_computation.38 | convolution fusion | flops 4300210176 | bytes 14682112 | tf_op jit(solution)/shard_map/dot_general | solution.py:101
  300.5 69.7 %reduce-scatter.5.cloned.1.call-done = bf16[1024,8,2,96]{0,3,1,2:T(8,128)(2,1)} async-done(((bf16[4096,8,2,96]{0,3,1,2:T(8,128)(2,1)}), bf16[1024,8,2,96]{0,3,1,2:T(8,128)(2,1)}) %reduce-scatter.5.cloned.1.call-update) | async-done | bytes 3145744 | tf_op jit(solution)/shard_map/reduce_scatter | solution.py:159
  370.2 1.8 fusion.64
  372.0 1.8 fusion.63
  373.8 1.8 fusion.62
  375.5 1.8 fusion.61
  377.3 1.8 fusion.60
  379.1 1.8 fusion.59
  380.9 1.9 fusion.58
  382.8 1.9 fusion.57
  384.7 5.6 %all-to-all-start.1 = ((bf16[8,1024,1,2,96]{1,4,3,2,0:T(8,128)(2,1)}), bf16[8,1024,1,2,96]{1,4,3,2,0:T(8,128)(2,1)S(1)}, u32[]{:S(2)}, u32[]{:S(2)}) async-start(bf16[8,1024,1,2,96]{1,4,3,2,0:T(8,128)(2,1)} %fusion.57), calls=%async_computation.3 | async-start | bytes 6291456 | tf_op jit(solution)/shard_map/all_to_all | solution.py:168
  391.0 69.9 %all-to-all-done.1 = bf16[8,1024,1,2,96]{1,4,3,2,0:T(8,128)(2,1)S(1)} async-done(((bf16[8,1024,1,2,96]{1,4,3,2,0:T(8,128)(2,1)}), bf16[8,1024,1,2,96]{1,4,3,2,0:T(8,128)(2,1)S(1)}, u32[]{:S(2)}, u32[]{:S(2)}) %all-to-all-start.1) | async-done | bytes 3145760 | tf_op jit(solution)/shard_map/all_to_all | solution.py:168
  460.9 5.4 %gather_fusion.1 = bf16[1024,1024]{1,0:T(8,128)(2,1)} fusion(bf16[1024,1536]{0,1:T(8,128)(2,1)S(1)} %bitcast.239, s32[1024]{0:T(1024)S(1)} %broadcast_clamp_fusion), kind=kCustom, calls=%fused_computation.1 | custom fusion | bytes 4198400 | tf_op jit(solution)/shard_map/jit(_take)/gather | solution.py:171
  466.2 2.7 gather.14
  469.0 9.4 %multiply_reduce_fusion = bf16[1024,512]{0,1:T(8,128)(2,1)} fusion(bf16[1024,512,2]{0,2,1:T(2,128)(2,1)S(1)} %gather.14, pred[512,2]{1,0:T(8,128)(4,1)S(1)} %copy.156, f32[512,2]{1,0:T(8,128)S(1)} %copy.166), kind=kLoop, calls=%fused_computation.44 | loop fusion | flops 3670016 | bytes 3150848 | tf_op jit(solution)/shard_map/reduce_sum | solution.py:173
  (178 shorter events, 15.8 us)
Async XLA Ops:
  7.2 18.6 %copy-start.6 = (f32[4096]{0:T(1024)S(1)}, f32[4096]{0:T(1024)}, u32[]{:S(2)}) copy-start(f32[4096]{0:T(1024)} %param.29) | copy-start | bytes 49156
  7.2 213.0 %all-gather.6.cloned.1.call-start = ((), (), s32[]{:S(2)}) async-start(), calls=%async_computation.5 | async-start | bytes 15728640 | tf_op jit(solution)/shard_map/all_gather | solution.py:151
  138.9 0.7 copy-start.9
  138.9 0.7 copy-start.10
  138.9 1.6 copy-start.5
  138.9 1.9 copy-start.3
  138.9 3.1 copy-start.2
  138.9 133.1 %all-gather.8.cloned.1.call-start = ((), (), s32[]{:S(2)}) async-start(), calls=%async_computation.7 | async-start | bytes 2359296 | tf_op jit(solution)/shard_map/all_gather | solution.py:14
  151.6 0.7 copy-start
  152.3 217.9 %reduce-scatter.5.cloned.1.call-start = ((), (), s32[]{:S(2)}) async-start(), calls=%async_computation.6 | async-start | bytes 15728640 | tf_op jit(solution)/shard_map/reduce_scatter | solution.py:159
  220.2 7.8 %copy-start.12 = (bf16[2,4096,256]{2,1,0:T(8,128)(2,1)S(1)}, bf16[2,4096,256]{2,1,0:T(8,128)(2,1)}, u32[]{:S(2)}) copy-start(bf16[2,4096,256]{2,1,0:T(8,128)(2,1)} %param.34) | copy-start | bytes 12582916
  228.0 8.7 %copy-start.1 = (bf16[2,256,4096]{2,1,0:T(8,128)(2,1)S(1)}, bf16[2,256,4096]{2,1,0:T(8,128)(2,1)}, u32[]{:S(2)}) copy-start(bf16[2,256,4096]{2,1,0:T(8,128)(2,1)} %param.35) | copy-start | bytes 12582916
  243.1 0.7 copy-start.15
  243.1 24.6 %copy-start.4 = (bf16[1024,256]{1,0:T(8,128)(2,1)S(1)}, bf16[1024,256]{1,0:T(8,128)(2,1)}, u32[]{:S(2)}) copy-start(bf16[1024,256]{1,0:T(8,128)(2,1)} %param.20) | copy-start | bytes 1572868
  243.1 235.3 %reduce-scatter.3.cloned.1.call-start = ((), (), s32[]{:S(2)}) async-start(), calls=%async_computation.4 | async-start | bytes 10485760 | tf_op jit(solution)/shard_map/reduce_scatter | solution.py:100
  287.5 4.0 copy-start.14
  290.2 2.5 copy-start.13
  384.7 5.9 %copy-start.7 = (s32[512,2]{0,1:T(2,128)S(1)}, s32[512,2]{0,1:T(2,128)}, u32[]{:S(2)}) copy-start(s32[512,2]{0,1:T(2,128)} %param.30) | copy-start | bytes 12292
  384.7 6.1 %copy-start.8 = (f32[512,2]{0,1:T(2,128)S(1)}, f32[512,2]{0,1:T(2,128)}, u32[]{:S(2)}) copy-start(f32[512,2]{0,1:T(2,128)} %param.32) | copy-start | bytes 12292
  384.7 6.2 %copy-start.11 = (f32[512]{0:T(512)S(1)}, f32[512]{0:T(512)}, u32[]{:S(2)}) copy-start(f32[512]{0:T(512)} %param.31) | copy-start | bytes 6148
  384.7 76.2 %all-to-all-start.1 = ((bf16[8,1024,1,2,96]{1,4,3,2,0:T(8,128)(2,1)}), bf16[8,1024,1,2,96]{1,4,3,2,0:T(8,128)(2,1)S(1)}, u32[]{:S(2)}, u32[]{:S(2)}) async-start(bf16[8,1024,1,2,96]{1,4,3,2,0:T(8,128)(2,1)} %fusion.57), calls=%async_computation.3 | async-start | bytes 6291456 | tf_op jit(solution)/shard_map/all_to_all | solution.py:168
Sparse Core Ops, SparseCore 0:
  139.0 81.0 all-gather.5
  222.3 49.7 all-gather.7
  274.6 95.5 reduce-scatter.4
  373.2 71.4 reduce-scatter.2
